TPU v7x, 512 devices: a 8x2x16 block of a 8x16x16 slice. The times are simulated.
512 devices in a mesh: grp: 2 (over y), kv: 16 (over z), tp: 16 (over x, core).
Axes of the slice: x: 8, y: 2, z: 16, core: 2. Of those that a mesh axis runs over, the one named last changes fastest.
The devices are a block of a 8x16x16 slice.
Arguments:
- tokens: bfloat16 [256, 4096], P('grp', ('kv', 'tp')), parts along dimension 0, may hold values from -8 to 8
- norm_gain: bfloat16 [4096], P('kv'), may hold values from 0.099609375 to 1.8984375
- w_query: bfloat16 [4096, 1024], P('kv', 'tp'), may hold values from -0.09375 to 0.09375
- w_key: bfloat16 [4096, 1024], P('kv', 'tp'), may hold values from -0.09375 to 0.09375
- w_value: bfloat16 [4096, 2048], P('kv', 'tp'), may hold values from -0.09375 to 0.09375
- w_ogate: bfloat16 [4096, 2048], P('kv', 'tp'), may hold values from -0.09375 to 0.09375
- w_igate: bfloat16 [4096, 16], P('kv', 'tp'), may hold values from -0.09375 to 0.09375
- w_fgate: bfloat16 [4096, 16], P('kv', 'tp'), may hold values from -0.09375 to 0.09375
- igate_bias: float32 [16], P('tp'), may hold values from -1 to 1
- fgate_bias: float32 [16], P('tp'), may hold values from -1 to 4
- state_c: float32 [256, 16, 64, 128], P(('grp', 'kv'), 'tp'), parts along dimension 0, may hold values from -1.5 to 1.5
- state_n: float32 [256, 16, 64], P(('grp', 'kv'), 'tp'), parts along dimension 0, may hold values from -1.5 to 1.5
- state_m: float32 [256, 16], P(('grp', 'kv'), 'tp'), parts along dimension 0, may hold values from -3 to 1
- head_gain: bfloat16 [16, 128], P('tp'), may hold values from 0.099609375 to 1.8984375
- w_out: bfloat16 [2048, 4096], P('tp', 'kv'), may hold values from -0.125 to 0.125
- ffn_gain: bfloat16 [4096], P('kv'), may hold values from 0.099609375 to 1.8984375
- w_gate: bfloat16 [4096, 11008], P('kv', 'tp'), may hold values from -0.09375 to 0.09375
- w_up: bfloat16 [4096, 11008], P('kv', 'tp'), may hold values from -0.09375 to 0.09375
- w_down: bfloat16 [11008, 4096], P('tp', 'kv'), may hold values from -0.0546875 to 0.0546875
Outputs:
- out_tokens: bfloat16 [256, 4096], P('grp', ('kv', 'tp')), parts along dimension 0
- new_c: float32 [256, 16, 64, 128], P(('grp', 'kv'), 'tp'), parts along dimension 0
- new_n: float32 [256, 16, 64], P(('grp', 'kv'), 'tp'), parts along dimension 0
- new_m: float32 [256, 16], P(('grp', 'kv'), 'tp'), parts along dimension 0
There are 2 independent parts, one for each index of `grp`. A program takes and returns all parts, laid end to end along the dimension named above; an argument that names none is the same for every part. Nothing has to cross between parts.
All inputs are finite; a program needn't handle non-finite values.
Results may differ from a plain program's by a relative error of at most 0.017.
Values may be sent and summed in bfloat16 or wider, within the bound.
No kernel may reach another device: no remote copies, remote signals or barrier semaphores. Data moves between devices by JAX's collectives and lax.ppermute only.
A program may use at most 64 MiB of HBM per device.

v0:
```python
import math
import jax
import jax.numpy as jnp
from jax import lax
from jax.sharding import PartitionSpec as P

D = 4096
DK = 64
DV = 128
norm_eps = 1e-06
igate_cap = 1.5


def split_up(value, dim, count):
    before, after = (value.shape[:dim], value.shape[dim + 1 :])
    return jnp.moveaxis(value.reshape(*before, count, -1, *after), dim, 0)


def summed_on_arrival(value, axis, dim):
    blocks = split_up(value, dim, lax.axis_size(axis))
    arrived = lax.all_to_all(blocks, axis, split_axis=0, concat_axis=0, tiled=True)
    return arrived.sum(axis=0)


def side_by_side(arrays, axis, dim, along):
    columns = [a.reshape(*a.shape[:along], -1) for a in arrays]
    both = jnp.concatenate(columns, axis=along)
    out, at, finished = (summed_on_arrival(both, axis, dim), 0, [])
    for a, column in zip(arrays, columns):
        section = out[..., at : at + column.shape[along]]
        finished.append(section.reshape(*section.shape[:along], *a.shape[along:]))
        at += column.shape[along]
    return tuple(finished)


def in_order(blocks, dim):
    lengths = list(blocks.shape[1:])
    lengths[dim] *= blocks.shape[0]
    return jnp.moveaxis(blocks, 0, dim).reshape(lengths)


def sent_to_all(value, axis):
    count = lax.axis_size(axis)
    return lax.all_to_all(
        jnp.broadcast_to(value[None], (count, *value.shape)), axis, 0, 0, tiled=True
    )


def gathered_copies(value, axis, dim):
    return in_order(sent_to_all(value, axis), dim)


def sum_at_owner(value, axis, dim):
    blocks = split_up(value, dim, lax.axis_size(axis))
    arrived = lax.all_to_all(blocks, axis, split_axis=0, concat_axis=0, tiled=True)
    return arrived.astype(jnp.float32).sum(axis=0)


def side_by_side_2(arrays, axis, dim, along):
    widths = [math.prod(a.shape[along:]) for a in arrays]
    both = jnp.concatenate(
        [a.reshape(*a.shape[:along], w) for a, w in zip(arrays, widths)], axis=along
    )
    out = sum_at_owner(both, axis, dim)
    blocks = jnp.split(out, [sum(widths[:k]) for k in range(1, len(widths))], axis=along)
    return tuple((b.reshape(*out.shape[:along], *a.shape[along:]) for a, b in zip(arrays, blocks)))


def cell_update(query, key_vec, value_vec, igate, fgate, state_c, state_n, state_m):
    carried = jax.nn.log_sigmoid(fgate) + state_m
    new_m = jnp.maximum(carried, igate)
    keep_weight = jnp.exp(carried - new_m)
    write_weight = jnp.exp(igate - new_m)
    new_c = (
        keep_weight[..., None, None] * state_c
        + write_weight[..., None, None] * key_vec[..., :, None] * value_vec[..., None, :]
    )
    new_n = keep_weight[..., None] * state_n + write_weight[..., None] * key_vec
    numerator = jnp.einsum("bhd,bhde->bhe", query, new_c, precision=lax.Precision.HIGHEST)
    denominator = jnp.sum(query * new_n, axis=-1)
    head_out = numerator / jnp.maximum(jnp.abs(denominator), jnp.exp(-new_m))[..., None]
    return (new_c, new_n, new_m, head_out)


def body(
    tokens,
    norm_gain,
    w_query,
    w_key,
    w_value,
    w_ogate,
    w_igate,
    w_fgate,
    igate_bias,
    fgate_bias,
    state_c,
    state_n,
    state_m,
    head_gain,
    w_out,
    ffn_gain,
    w_gate,
    w_up,
    w_down,
):
    seq_rows = state_c.shape[0]
    heads_here = state_c.shape[1]
    token_cols = lax.all_gather(tokens, "tp", axis=1, tiled=True)
    token_vals = token_cols.astype(jnp.float32)
    normed = (token_vals * norm_gain.astype(jnp.float32)).astype(jnp.bfloat16)
    squares = jnp.sum(token_vals * token_vals, axis=1)
    part_query = jnp.dot(normed, w_query, preferred_element_type=jnp.float32)
    part_key = jnp.dot(normed, w_key, preferred_element_type=jnp.float32)
    part_value = jnp.dot(normed, w_value, preferred_element_type=jnp.float32)
    part_ogate = jnp.dot(normed, w_ogate, preferred_element_type=jnp.float32)
    part_igate = jnp.dot(normed, w_igate, preferred_element_type=jnp.float32)
    part_fgate = jnp.dot(normed, w_fgate, preferred_element_type=jnp.float32)
    sum_query, sum_key, sum_value, sum_ogate, sum_igate, sum_fgate, sum_squares = side_by_side(
        (part_query, part_key, part_value, part_ogate, part_igate, part_fgate, squares), "kv", 0, 1
    )
    row_scale = lax.rsqrt(sum_squares / D + norm_eps)[:, None]
    query = (row_scale * sum_query).reshape(seq_rows, heads_here, DK)
    key_vec = (row_scale * sum_key).reshape(seq_rows, heads_here, DK) * DK ** (-0.5)
    value_vec = (row_scale * sum_value).reshape(seq_rows, heads_here, DV)
    ogate = (row_scale * sum_ogate).reshape(seq_rows, heads_here, DV)
    igate = igate_cap * jnp.tanh((row_scale * sum_igate + igate_bias) / igate_cap)
    fgate = row_scale * sum_fgate + fgate_bias
    new_c, new_n, new_m, head_out = cell_update(
        query, key_vec, value_vec, igate, fgate, state_c, state_n, state_m
    )
    merged = (
        (head_out * head_gain.astype(jnp.float32) * jax.nn.sigmoid(ogate))
        .reshape(seq_rows, heads_here * DV)
        .astype(jnp.bfloat16)
    )
    attn_part = jnp.dot(gathered_copies(merged, "kv", 0), w_out, preferred_element_type=jnp.float32)
    attn_out = sum_at_owner(attn_part.astype(jnp.bfloat16), "tp", 1)
    middle = (tokens.astype(jnp.float32) + attn_out).astype(jnp.bfloat16)
    middle_cols = lax.all_gather(middle, "tp", axis=1, tiled=True)
    middle_vals = middle_cols.astype(jnp.float32)
    normed_two = (middle_vals * ffn_gain.astype(jnp.float32)).astype(jnp.bfloat16)
    squares_two = jnp.sum(middle_vals * middle_vals, axis=1)
    gate_part = jnp.dot(normed_two, w_gate, preferred_element_type=jnp.float32)
    up_part = jnp.dot(normed_two, w_up, preferred_element_type=jnp.float32)
    gate_sum, up_sum, total_two = side_by_side_2(
        (
            gate_part.astype(jnp.bfloat16),
            up_part.astype(jnp.bfloat16),
            squares_two.astype(jnp.bfloat16),
        ),
        "kv",
        0,
        1,
    )
    ffn_scale = lax.rsqrt(total_two / D + norm_eps)[:, None]
    hidden = (jax.nn.silu(ffn_scale * gate_sum) * (ffn_scale * up_sum)).astype(jnp.bfloat16)
    down_part = jnp.dot(
        gathered_copies(hidden, "kv", 0), w_down, preferred_element_type=jnp.float32
    )
    down_out = sum_at_owner(down_part.astype(jnp.bfloat16), "tp", 1)
    out_tokens = (middle.astype(jnp.float32) + down_out).astype(jnp.bfloat16)
    return (out_tokens, new_c, new_n, new_m)


def solution(mesh):
    placed = (
        P("grp", ("kv", "tp")),
        P("kv"),
        P("kv", "tp"),
        P("kv", "tp"),
        P("kv", "tp"),
        P("kv", "tp"),
        P("kv", "tp"),
        P("kv", "tp"),
        P("tp"),
        P("tp"),
        P(("grp", "kv"), "tp", None, None),
        P(("grp", "kv"), "tp", None),
        P(("grp", "kv"), "tp"),
        P("tp", None),
        P("tp", "kv"),
        P("kv"),
        P("kv", "tp"),
        P("kv", "tp"),
        P("tp", "kv"),
    )
    return jax.shard_map(
        body,
        mesh=mesh,
        in_specs=placed,
        out_specs=(
            P("grp", ("kv", "tp")),
            P(("grp", "kv"), "tp", None, None),
            P(("grp", "kv"), "tp", None),
            P(("grp", "kv"), "tp"),
        ),
        check_vma=False,
    )
```

profile of v0, /device:TPU:65, one launch (start us, length us, event | category | flops | bytes accessed | tf_op | source)
XLA Modules:
  0.0 202.4 jit_solution(7340011110046809596)
XLA Ops:
  0.6 0.0 copy-start
  0.6 0.7 convert_element_type.76
  1.4 55.9 %all_gather.6 = bf16[128,256]{0,1:T(8,128)(2,1)S(1)} all-gather(bf16[128,16]{0,1:T(8,128)(2,1)} %param.19), channel_id=1, replica_groups=mesh['grp'=2,'kv'=16,'tp'=16] {'tp'}, dimensions={1}, use_global_device_ids=true | all-gather | bytes 69632 | tf_op jit(solution)/shard_map/all_gather | solution.py:108
  57.3 0.1 copy.69
  57.4 0.1 fusion.4
  57.5 0.0 copy-start.8
  57.5 0.2 concatenate.31
  57.7 0.6 copy-done.8
  58.3 0.1 convolution_bitcast_fusion.4
  58.4 0.7 copy-done.5
  59.1 0.1 convolution_bitcast_fusion.3
  59.3 0.7 copy-done.6
  60.0 0.1 convolution_bitcast_fusion.2
  60.1 0.5 copy-done.12
  60.6 0.1 convolution_bitcast_fusion.1
  60.8 0.5 copy-done.13
  61.3 0.1 convolution_bitcast_fusion
  61.5 0.6 copy-done.9
  62.1 0.1 convolution_bitcast_fusion.5
  62.2 0.9 concatenate.27
  63.1 7.2 %all-to-all-start = ((f32[16,8,387]{2,1,0:T(8,128)}), f32[16,8,387]{2,1,0:T(8,128)S(1)}, u32[]{:S(2)}, u32[]{:S(2)}) async-start(f32[16,8,387]{2,1,0:T(8,128)} %concatenate.27), calls=%async_computation | async-start | bytes 524288 | tf_op jit(solution)/shard_map/all_to_all | solution.py:21
  70.3 0.0 copy-start.4
  71.6 0.0 copy-done.14
  71.7 0.1 copy.75
  71.7 0.0 copy-done.15
  71.7 12.5 %all-to-all-done = f32[16,8,387]{2,1,0:T(8,128)S(1)} async-done(((f32[16,8,387]{2,1,0:T(8,128)}), f32[16,8,387]{2,1,0:T(8,128)S(1)}, u32[]{:S(2)}, u32[]{:S(2)}) %all-to-all-start) | async-done | bytes 198176 | tf_op jit(solution)/shard_map/all_to_all | solution.py:21
  84.3 0.3 multiply_reduce_fusion
  84.5 0.1 slice_multiply_fusion.4
  84.6 0.7 copy-done.11
  85.3 0.8 fusion.39
  86.1 0.1 copy.77
  86.2 0.1 maximum_reduce_fusion
  86.3 0.1 multiply_add_fusion
  86.4 0.0 copy-start.1
  86.5 0.3 fusion
  86.8 0.1 fusion.40
  86.9 21.4 %all_to_all.30 = bf16[16,8,128]{2,1,0:T(8,128)(2,1)S(1)} all-to-all(bf16[16,8,128]{2,1,0:T(8,128)(2,1)S(1)} %broadcast_in_dim.4), channel_id=1, replica_groups=mesh['grp'=2,'kv'=16,'tp'=16] {'kv'}, dimensions={0} | all-to-all | bytes 65536 | tf_op jit(solution)/shard_map/all_to_all | solution.py:44
  108.3 0.1 convolution_convert_fusion.3
  108.4 0.7 copy.78
  109.1 6.3 %all-to-all-start.2 = ((bf16[16,128,16]{1,2,0:T(8,128)(2,1)}), bf16[16,128,16]{1,2,0:T(8,128)(2,1)S(1)}, u32[]{:S(2)}, u32[]{:S(2)}) async-start(bf16[16,128,16]{1,2,0:T(8,128)(2,1)} %bitcast.23), calls=%async_computation.2 | async-start | bytes 131072 | tf_op jit(solution)/shard_map/all_to_all | solution.py:55
  115.5 0.0 copy-start.10
  115.5 7.7 %all-to-all-done.2 = bf16[16,128,16]{1,2,0:T(8,128)(2,1)S(1)} async-done(((bf16[16,128,16]{1,2,0:T(8,128)(2,1)}), bf16[16,128,16]{1,2,0:T(8,128)(2,1)S(1)}, u32[]{:S(2)}, u32[]{:S(2)}) %all-to-all-start.2) | async-done | bytes 65568 | tf_op jit(solution)/shard_map/all_to_all | solution.py:55
  123.3 15.0 %all_gather.7 = bf16[128,256]{0,1:T(8,128)(2,1)S(1)} all-gather(bf16[128,16]{0,1:T(8,128)(2,1)S(1)} %add_convert_fusion.1), channel_id=1, replica_groups=mesh['grp'=2,'kv'=16,'tp'=16] {'tp'}, dimensions={1}, use_global_device_ids=true | all-gather | bytes 69632 | tf_op jit(solution)/shard_map/all_gather | solution.py:139
  138.2 0.1 fusion.6
  138.3 0.2 convert_element_type.95
  138.5 0.0 copy-start.2
  138.5 0.3 convolution_convert_fusion.1
  138.9 0.1 copy.79
  139.0 0.5 copy-done.2
  139.5 0.3 convolution_convert_fusion
  139.8 0.1 copy.80
  140.0 0.2 concatenate.30
  140.2 21.4 %all_to_all.31 = bf16[16,8,1377]{2,1,0:T(8,128)(2,1)S(1)} all-to-all(bf16[16,8,1377]{2,1,0:T(8,128)(2,1)S(1)} %concatenate.30), channel_id=1, replica_groups=mesh['grp'=2,'kv'=16,'tp'=16] {'kv'}, dimensions={0} | all-to-all | bytes 705024 | tf_op jit(solution)/shard_map/all_to_all | solution.py:55
  161.6 0.1 convert_reduce_fusion
  161.7 0.0 copy-start.3
  161.7 0.2 fusion.24
  161.9 0.1 fusion.13
  162.0 22.1 %all_to_all.32 = bf16[16,8,688]{2,1,0:T(8,128)(2,1)S(1)} all-to-all(bf16[16,8,688]{2,1,0:T(8,128)(2,1)S(1)} %broadcast_in_dim.5), channel_id=1, replica_groups=mesh['grp'=2,'kv'=16,'tp'=16] {'kv'}, dimensions={0} | all-to-all | bytes 352256 | tf_op jit(solution)/shard_map/all_to_all | solution.py:44
  184.1 0.2 convolution_convert_fusion.2
  184.3 0.7 copy.82
  185.0 8.9 %all-to-all-start.5 = ((bf16[16,128,16]{1,2,0:T(8,128)(2,1)}), bf16[16,128,16]{1,2,0:T(8,128)(2,1)S(1)}, u32[]{:S(2)}, u32[]{:S(2)}) async-start(bf16[16,128,16]{1,2,0:T(8,128)(2,1)} %bitcast.28), calls=%async_computation.5 | async-start | bytes 131072 | tf_op jit(solution)/shard_map/all_to_all | solution.py:55
  194.0 0.6 copy.84
  194.6 7.2 %all-to-all-done.5 = bf16[16,128,16]{1,2,0:T(8,128)(2,1)S(1)} async-done(((bf16[16,128,16]{1,2,0:T(8,128)(2,1)}), bf16[16,128,16]{1,2,0:T(8,128)(2,1)S(1)}, u32[]{:S(2)}, u32[]{:S(2)}) %all-to-all-start.5) | async-done | bytes 65568 | tf_op jit(solution)/shard_map/all_to_all | solution.py:55
  201.8 0.6 add_convert_fusion
  (26 shorter events, 0.1 us)
Async XLA Ops:
  0.6 137.9 %copy-start = (bf16[256,688]{0,1:T(8,128)(2,1)S(1)}, bf16[256,688]{0,1:T(8,128)(2,1)}, u32[]{:S(2)}) copy-start(bf16[256,688]{0,1:T(8,128)(2,1)} %param.35) | copy-start | bytes 1056772
  57.5 0.8 copy-start.8
  58.3 0.8 copy-start.5
  59.1 0.8 copy-start.6
  60.0 0.7 copy-start.12
  60.6 0.7 copy-start.13
  61.3 0.8 copy-start.9
  63.1 8.6 %copy-start.14 = (f32[8,1]{0,1:T(1,128)S(1)}, f32[8,1]{0,1:T(1,128)}, u32[]{:S(2)}) copy-start(f32[8,1]{0,1:T(1,128)} %param.31) | copy-start | bytes 100
  63.1 8.7 %copy-start.15 = (bf16[1,128]{1,0:T(2,128)(2,1)S(1)}, bf16[1,128]{1,0:T(2,128)(2,1)}, u32[]{:S(2)}) copy-start(bf16[1,128]{1,0:T(2,128)(2,1)} %param.32) | copy-start | bytes 772
  63.1 21.2 %all-to-all-start = ((f32[16,8,387]{2,1,0:T(8,128)}), f32[16,8,387]{2,1,0:T(8,128)S(1)}, u32[]{:S(2)}, u32[]{:S(2)}) async-start(f32[16,8,387]{2,1,0:T(8,128)} %concatenate.27), calls=%async_computation | async-start | bytes 524288 | tf_op jit(solution)/shard_map/all_to_all | solution.py:21
  70.3 16.0 %copy-start.4 = (f32[8,1,64,128]{3,2,1,0:T(8,128)S(1)}, f32[8,1,64,128]{3,2,1,0:T(8,128)}, u32[]{:S(2)}) copy-start(f32[8,1,64,128]{3,2,1,0:T(8,128)} %param.29) | copy-start | bytes 786436
  84.6 0.7 copy-start.11
  86.4 22.0 %copy-start.1 = (f32[8,1,64,128]{3,2,1,0:T(8,128)}, f32[8,1,64,128]{3,2,1,0:T(8,128)S(1)}, u32[]{:S(2)}) copy-start(f32[8,1,64,128]{3,2,1,0:T(8,128)S(1)} %multiply_add_fusion) | copy-start | bytes 786436
  86.8 21.5 %copy-start.7 = (bf16[128,256]{1,0:T(8,128)(2,1)S(1)}, bf16[128,256]{1,0:T(8,128)(2,1)}, u32[]{:S(2)}) copy-start(bf16[128,256]{1,0:T(8,128)(2,1)} %param.33) | copy-start | bytes 196612
  109.1 6.3 %copy-start.16 = (bf16[256]{0:T(256)(128)(2,1)S(1)}, bf16[256]{0:T(256)(128)(2,1)}, u32[]{:S(2)}) copy-start(bf16[256]{0:T(256)(128)(2,1)} %param.34) | copy-start | bytes 1540
  109.1 14.1 %all-to-all-start.2 = ((bf16[16,128,16]{1,2,0:T(8,128)(2,1)}), bf16[16,128,16]{1,2,0:T(8,128)(2,1)S(1)}, u32[]{:S(2)}, u32[]{:S(2)}) async-start(bf16[16,128,16]{1,2,0:T(8,128)(2,1)} %bitcast.23), calls=%async_computation.2 | async-start | bytes 131072 | tf_op jit(solution)/shard_map/all_to_all | solution.py:55
  115.5 7.8 %copy-start.10 = (bf16[128,16]{0,1:T(8,128)(2,1)S(1)}, bf16[128,16]{0,1:T(8,128)(2,1)}, u32[]{:S(2)}) copy-start(bf16[128,16]{0,1:T(8,128)(2,1)} %param.19) | copy-start | bytes 12292
  138.5 1.0 copy-start.2
  161.7 22.4 %copy-start.3 = (bf16[688,256]{1,0:T(8,128)(2,1)S(1)}, bf16[688,256]{1,0:T(8,128)(2,1)}, u32[]{:S(2)}) copy-start(bf16[688,256]{1,0:T(8,128)(2,1)} %param.37) | copy-start | bytes 1056772
  185.0 16.7 %all-to-all-start.5 = ((bf16[16,128,16]{1,2,0:T(8,128)(2,1)}), bf16[16,128,16]{1,2,0:T(8,128)(2,1)S(1)}, u32[]{:S(2)}, u32[]{:S(2)}) async-start(bf16[16,128,16]{1,2,0:T(8,128)(2,1)} %bitcast.28), calls=%async_computation.5 | async-start | bytes 131072 | tf_op jit(solution)/shard_map/all_to_all | solution.py:55
where the time goes:
time: 203 us; the launch traced here: 202 us
  blocking collectives  136 us (67%)
  waiting for transfers between devices  27.4 us (13%)
  starting transfers between devices  22.5 us (11%)
  local copies, waits for them, and re-layouts  9 us (4%)
  other arithmetic  3.32 us (2%)
  between operations  2.24 us (1%)
  matrix products  2.09 us (1%)
    all_gather x1, blocking collectives, body(): token_cols = lax.all_gather(tokens, 'tp', axis=1, tiled=True)  55.9 us
    all_to_all x2, blocking collectives, sent_to_all(): lax.all_to_all(jnp.broadcast_to(value[None], (count, *value.shape)), axis...  43.5 us
    all_to_all x1, blocking collectives, sum_at_owner(): lax.all_to_all(blocks, axis, split_axis=0, concat_axis=0, tiled=True)  21.4 us
    all_to_all x2, starting transfers between devices, sum_at_owner(): lax.all_to_all(blocks, axis, split_axis=0, concat_axis=0, tiled=True)  15.3 us
    all_gather x1, blocking collectives, body(): middle_cols = lax.all_gather(middle, 'tp', axis=1, tiled=True)  15 us
    all_to_all x2, waiting for transfers between devices, sum_at_owner(): lax.all_to_all(blocks, axis, split_axis=0, concat_axis=0, tiled=True)  14.9 us
    all_to_all x1, waiting for transfers between devices, summed_on_arrival(): lax.all_to_all(blocks, axis, split_axis=0, concat_axis=0, tiled=True)  12.5 us
    all_to_all x1, starting transfers between devices, summed_on_arrival(): lax.all_to_all(blocks, axis, split_axis=0, concat_axis=0, tiled=True)  7.23 us
  transfers between devices with their start and end apart: 3, of which 3 were waited for; matrix products, arithmetic and copies ran while one was open for 0% of the time, Pallas kernels for 0%

commit v1 on v0

--- a/solution.py
+++ b/solution.py
@@ -105,7 +105,11 @@
 ):
     seq_rows = state_c.shape[0]
     heads_here = state_c.shape[1]
-    token_cols = lax.all_gather(tokens, "tp", axis=1, tiled=True)
+    size = lax.axis_size("tp")
+    repeats = [size if d == 1 else 1 for d in range(tokens.ndim)]
+    token_cols = lax.all_to_all(
+        jnp.tile(tokens, repeats), "tp", split_axis=1, concat_axis=1, tiled=True
+    )
     token_vals = token_cols.astype(jnp.float32)
     normed = (token_vals * norm_gain.astype(jnp.float32)).astype(jnp.bfloat16)
     squares = jnp.sum(token_vals * token_vals, axis=1)

time: 203 us -> 202 us (level)
  blocking collectives: 136 us -> 79.8 us
  starting transfers between devices: 22.5 us -> 66.6 us
  waiting for transfers between devices: 27.4 us -> 35.5 us
  local copies, waits for them, and re-layouts: 9 us -> 12 us
    all_gather x1 -> x0, blocking collectives: 55.9 us -> none  [body(): token_cols = lax.all_gather(tokens, 'tp', axis=1, tiled=True)]
    all_to_all x0 -> x1, starting transfers between devices: none -> 44.9 us  [body(): lax.all_to_all(jnp.tile(tokens, repeats), 'tp', split_axis=1, concat_axis...]
    all_to_all x0 -> x1, waiting for transfers between devices: none -> 7.82 us  [body(): lax.all_to_all(jnp.tile(tokens, repeats), 'tp', split_axis=1, concat_axis...]
    unnamed x36 -> x38, local copies, waits for them, and re-layouts: 5.57 us -> 5.45 us
  transfers between devices with their start and end apart: 3 -> 4, of which waited for: 3 -> 4; matrix products, arithmetic and copies ran while one was open for 0% -> 0% of each run, Pallas kernels for 0% -> 0%
where the time goes in v1:
time: 202 us; the launch traced here: 201 us
  blocking collectives  79.8 us (40%)
  starting transfers between devices  66.6 us (33%)
  waiting for transfers between devices  35.5 us (18%)
  local copies, waits for them, and re-layouts  12 us (6%)
  other arithmetic  2.64 us (1%)
  between operations  2.23 us (1%)
  matrix products  2.09 us (1%)
    all_to_all x1, starting transfers between devices, body(): lax.all_to_all(jnp.tile(tokens, repeats), 'tp', split_axis=1, concat_axis...  44.9 us
    all_to_all x2, blocking collectives, sent_to_all(): lax.all_to_all(jnp.broadcast_to(value[None], (count, *value.shape)), axis...  43.4 us
    all_to_all x1, blocking collectives, sum_at_owner(): lax.all_to_all(blocks, axis, split_axis=0, concat_axis=0, tiled=True)  21.4 us
    all_to_all x2, waiting for transfers between devices, sum_at_owner(): lax.all_to_all(blocks, axis, split_axis=0, concat_axis=0, tiled=True)  15.1 us
    all_gather x1, blocking collectives, body(): middle_cols = lax.all_gather(middle, 'tp', axis=1, tiled=True)  14.9 us
    all_to_all x2, starting transfers between devices, sum_at_owner(): lax.all_to_all(blocks, axis, split_axis=0, concat_axis=0, tiled=True)  14.3 us
    all_to_all x1, waiting for transfers between devices, summed_on_arrival(): lax.all_to_all(blocks, axis, split_axis=0, concat_axis=0, tiled=True)  12.6 us
    all_to_all x1, waiting for transfers between devices, body(): lax.all_to_all(jnp.tile(tokens, repeats), 'tp', split_axis=1, concat_axis...  7.82 us
  transfers between devices with their start and end apart: 4, of which 4 were waited for; matrix products, arithmetic and copies ran while one was open for 0% of the time, Pallas kernels for 0%

profile of v1, /device:TPU:65, one launch (start us, length us, event | category | flops | bytes accessed | tf_op | source)
XLA Modules:
  0.0 200.8 jit_solution(3735989059813873766)
XLA Ops:
  0.6 0.0 copy-start
  0.6 1.4 tile.2
  2.0 44.9 %all-to-all-start = ((bf16[128,16,16]{0,2,1:T(8,128)(2,1)}), bf16[128,16,16]{0,2,1:T(8,128)(2,1)S(1)}, u32[]{:S(2)}, u32[]{:S(2)}) async-start(bf16[128,16,16]{0,2,1:T(8,128)(2,1)} %tile.2), calls=%async_computation | async-start | bytes 131072 | tf_op jit(solution)/shard_map/all_to_all | solution.py:110
  46.9 0.1 mul.185
  47.0 7.8 %all-to-all-done = bf16[128,16,16]{0,2,1:T(8,128)(2,1)S(1)} async-done(((bf16[128,16,16]{0,2,1:T(8,128)(2,1)}), bf16[128,16,16]{0,2,1:T(8,128)(2,1)S(1)}, u32[]{:S(2)}, u32[]{:S(2)}) %all-to-all-start) | async-done | bytes 65568 | tf_op jit(solution)/shard_map/all_to_all | solution.py:110
  54.8 0.4 copy.65
  55.3 0.4 reshape.211
  55.7 0.7 copy-done.8
  56.5 0.1 fusion.10
  56.6 0.6 copy-done.9
  57.2 0.1 fusion.12
  57.3 0.7 copy-done.5
  58.1 0.1 fusion.5
  58.2 0.7 copy-done.6
  58.9 0.1 fusion.7
  59.0 0.1 multiply_reduce_fusion
  59.2 0.4 copy.66
  59.6 0.0 copy-start.12
  59.6 0.5 dot_general.43
  60.1 0.2 copy-done.12
  60.3 0.1 convolution_bitcast_fusion
  60.4 0.6 copy-done.13
  61.0 0.1 convolution_bitcast_fusion.1
  61.1 0.2 concatenate.19
  61.3 0.8 concatenate.15
  62.1 7.4 %all-to-all-start.1 = ((f32[16,8,387]{2,1,0:T(8,128)}), f32[16,8,387]{2,1,0:T(8,128)S(1)}, u32[]{:S(2)}, u32[]{:S(2)}) async-start(f32[16,8,387]{2,1,0:T(8,128)} %concatenate.15), calls=%async_computation.1 | async-start | bytes 524288 | tf_op jit(solution)/shard_map/all_to_all | solution.py:21
  69.6 0.0 copy-start.4
  69.6 0.1 copy.70
  71.0 12.6 %all-to-all-done.1 = f32[16,8,387]{2,1,0:T(8,128)S(1)} async-done(((f32[16,8,387]{2,1,0:T(8,128)}), f32[16,8,387]{2,1,0:T(8,128)S(1)}, u32[]{:S(2)}, u32[]{:S(2)}) %all-to-all-start.1) | async-done | bytes 198176 | tf_op jit(solution)/shard_map/all_to_all | solution.py:21
  83.6 0.3 multiply_reduce_fusion.1
  83.8 0.1 slice_multiply_fusion.4
  83.9 0.7 copy-done.11
  84.6 0.8 fusion.37
  85.4 0.1 copy.72
  85.5 0.1 maximum_reduce_fusion
  85.6 0.1 multiply_add_fusion
  85.7 0.0 copy-start.1
  85.7 0.3 fusion
  86.1 0.1 fusion.38
  86.2 21.4 %all_to_all.36 = bf16[16,8,128]{2,1,0:T(8,128)(2,1)S(1)} all-to-all(bf16[16,8,128]{2,1,0:T(8,128)(2,1)S(1)} %broadcast_in_dim.4), channel_id=1, replica_groups=mesh['grp'=2,'kv'=16,'tp'=16] {'kv'}, dimensions={0} | all-to-all | bytes 65536 | tf_op jit(solution)/shard_map/all_to_all | solution.py:44
  107.5 0.1 convolution_convert_fusion.3
  107.7 0.7 copy.73
  108.4 5.4 %all-to-all-start.3 = ((bf16[16,128,16]{1,2,0:T(8,128)(2,1)}), bf16[16,128,16]{1,2,0:T(8,128)(2,1)S(1)}, u32[]{:S(2)}, u32[]{:S(2)}) async-start(bf16[16,128,16]{1,2,0:T(8,128)(2,1)} %bitcast.22), calls=%async_computation.3 | async-start | bytes 131072 | tf_op jit(solution)/shard_map/all_to_all | solution.py:55
  113.8 7.9 %all-to-all-done.3 = bf16[16,128,16]{1,2,0:T(8,128)(2,1)S(1)} async-done(((bf16[16,128,16]{1,2,0:T(8,128)(2,1)}), bf16[16,128,16]{1,2,0:T(8,128)(2,1)S(1)}, u32[]{:S(2)}, u32[]{:S(2)}) %all-to-all-start.3) | async-done | bytes 65568 | tf_op jit(solution)/shard_map/all_to_all | solution.py:55
  121.7 14.9 %all_gather.3 = bf16[128,256]{0,1:T(8,128)(2,1)S(1)} all-gather(bf16[128,16]{0,1:T(8,128)(2,1)S(1)} %add_convert_fusion.1), channel_id=1, replica_groups=mesh['grp'=2,'kv'=16,'tp'=16] {'tp'}, dimensions={1}, use_global_device_ids=true | all-gather | bytes 69632 | tf_op jit(solution)/shard_map/all_gather | solution.py:143
  136.7 0.1 fusion.4
  136.7 0.3 convolution_convert_fusion.1
  137.1 0.1 copy.74
  137.2 0.5 copy-done.2
  137.7 0.3 convolution_convert_fusion
  138.0 0.1 copy.75
  138.2 0.2 convert_element_type.119
  138.4 0.2 concatenate.18
  138.6 21.4 %all_to_all.37 = bf16[16,8,1377]{2,1,0:T(8,128)(2,1)S(1)} all-to-all(bf16[16,8,1377]{2,1,0:T(8,128)(2,1)S(1)} %concatenate.18), channel_id=1, replica_groups=mesh['grp'=2,'kv'=16,'tp'=16] {'kv'}, dimensions={0} | all-to-all | bytes 705024 | tf_op jit(solution)/shard_map/all_to_all | solution.py:55
  160.1 0.1 convert_reduce_fusion
  160.1 0.2 fusion.22
  160.3 0.1 fusion.17
  160.4 22.1 %all_to_all.38 = bf16[16,8,688]{2,1,0:T(8,128)(2,1)S(1)} all-to-all(bf16[16,8,688]{2,1,0:T(8,128)(2,1)S(1)} %broadcast_in_dim.5), channel_id=1, replica_groups=mesh['grp'=2,'kv'=16,'tp'=16] {'kv'}, dimensions={0} | all-to-all | bytes 352256 | tf_op jit(solution)/shard_map/all_to_all | solution.py:44
  182.5 0.2 convolution_convert_fusion.2
  182.8 0.7 copy.77
  183.5 9.0 %all-to-all-start.6 = ((bf16[16,128,16]{1,2,0:T(8,128)(2,1)}), bf16[16,128,16]{1,2,0:T(8,128)(2,1)S(1)}, u32[]{:S(2)}, u32[]{:S(2)}) async-start(bf16[16,128,16]{1,2,0:T(8,128)(2,1)} %bitcast.27), calls=%async_computation.6 | async-start | bytes 131072 | tf_op jit(solution)/shard_map/all_to_all | solution.py:55
  192.4 0.6 copy.79
  193.0 7.2 %all-to-all-done.6 = bf16[16,128,16]{1,2,0:T(8,128)(2,1)S(1)} async-done(((bf16[16,128,16]{1,2,0:T(8,128)(2,1)}), bf16[16,128,16]{1,2,0:T(8,128)(2,1)S(1)}, u32[]{:S(2)}, u32[]{:S(2)}) %all-to-all-start.6) | async-done | bytes 65568 | tf_op jit(solution)/shard_map/all_to_all | solution.py:55
  200.2 0.6 add_convert_fusion
  (35 shorter events, 0.2 us)
Async XLA Ops:
  0.6 136.1 %copy-start = (bf16[256,688]{0,1:T(8,128)(2,1)S(1)}, bf16[256,688]{0,1:T(8,128)(2,1)}, u32[]{:S(2)}) copy-start(bf16[256,688]{0,1:T(8,128)(2,1)} %param.35) | copy-start | bytes 1056772
  2.0 44.9 %copy-start.14 = (bf16[256]{0:T(256)(128)(2,1)S(1)}, bf16[256]{0:T(256)(128)(2,1)}, u32[]{:S(2)}) copy-start(bf16[256]{0:T(256)(128)(2,1)} %param.20) | copy-start | bytes 1540
  2.0 52.8 %all-to-all-start = ((bf16[128,16,16]{0,2,1:T(8,128)(2,1)}), bf16[128,16,16]{0,2,1:T(8,128)(2,1)S(1)}, u32[]{:S(2)}, u32[]{:S(2)}) async-start(bf16[128,16,16]{0,2,1:T(8,128)(2,1)} %tile.2), calls=%async_computation | async-start | bytes 131072 | tf_op jit(solution)/shard_map/all_to_all | solution.py:110
  55.7 0.8 copy-start.8
  56.5 0.8 copy-start.9
  57.2 0.8 copy-start.5
  58.1 0.8 copy-start.6
  59.6 0.7 copy-start.12
  60.3 0.7 copy-start.13
  62.1 7.4 %copy-start.15 = (f32[8,1]{0,1:T(1,128)S(1)}, f32[8,1]{0,1:T(1,128)}, u32[]{:S(2)}) copy-start(f32[8,1]{0,1:T(1,128)} %param.31) | copy-start | bytes 100
  62.1 8.8 %copy-start.16 = (bf16[1,128]{1,0:T(2,128)(2,1)S(1)}, bf16[1,128]{1,0:T(2,128)(2,1)}, u32[]{:S(2)}) copy-start(bf16[1,128]{1,0:T(2,128)(2,1)} %param.32) | copy-start | bytes 772
  62.1 21.4 %all-to-all-start.1 = ((f32[16,8,387]{2,1,0:T(8,128)}), f32[16,8,387]{2,1,0:T(8,128)S(1)}, u32[]{:S(2)}, u32[]{:S(2)}) async-start(f32[16,8,387]{2,1,0:T(8,128)} %concatenate.15), calls=%async_computation.1 | async-start | bytes 524288 | tf_op jit(solution)/shard_map/all_to_all | solution.py:21
  69.6 16.0 %copy-start.4 = (f32[8,1,64,128]{3,2,1,0:T(8,128)S(1)}, f32[8,1,64,128]{3,2,1,0:T(8,128)}, u32[]{:S(2)}) copy-start(f32[8,1,64,128]{3,2,1,0:T(8,128)} %param.29) | copy-start | bytes 786436
  83.9 0.7 copy-start.11
  85.7 21.9 %copy-start.1 = (f32[8,1,64,128]{3,2,1,0:T(8,128)}, f32[8,1,64,128]{3,2,1,0:T(8,128)S(1)}, u32[]{:S(2)}) copy-start(f32[8,1,64,128]{3,2,1,0:T(8,128)S(1)} %multiply_add_fusion) | copy-start | bytes 786436
  86.1 21.5 %copy-start.7 = (bf16[128,256]{1,0:T(8,128)(2,1)S(1)}, bf16[128,256]{1,0:T(8,128)(2,1)}, u32[]{:S(2)}) copy-start(bf16[128,256]{1,0:T(8,128)(2,1)} %param.33) | copy-start | bytes 196612
  108.4 5.4 %copy-start.17 = (bf16[256]{0:T(256)(128)(2,1)S(1)}, bf16[256]{0:T(256)(128)(2,1)}, u32[]{:S(2)}) copy-start(bf16[256]{0:T(256)(128)(2,1)} %param.34) | copy-start | bytes 1540
  108.4 13.3 %all-to-all-start.3 = ((bf16[16,128,16]{1,2,0:T(8,128)(2,1)}), bf16[16,128,16]{1,2,0:T(8,128)(2,1)S(1)}, u32[]{:S(2)}, u32[]{:S(2)}) async-start(bf16[16,128,16]{1,2,0:T(8,128)(2,1)} %bitcast.22), calls=%async_computation.3 | async-start | bytes 131072 | tf_op jit(solution)/shard_map/all_to_all | solution.py:55
  113.8 7.9 %copy-start.10 = (bf16[128,16]{0,1:T(8,128)(2,1)S(1)}, bf16[128,16]{0,1:T(8,128)(2,1)}, u32[]{:S(2)}) copy-start(bf16[128,16]{0,1:T(8,128)(2,1)} %param.19) | copy-start | bytes 12292
  136.7 1.0 copy-start.2
  160.1 22.4 %copy-start.3 = (bf16[688,256]{1,0:T(8,128)(2,1)S(1)}, bf16[688,256]{1,0:T(8,128)(2,1)}, u32[]{:S(2)}) copy-start(bf16[688,256]{1,0:T(8,128)(2,1)} %param.37) | copy-start | bytes 1056772
  183.5 16.7 %all-to-all-start.6 = ((bf16[16,128,16]{1,2,0:T(8,128)(2,1)}), bf16[16,128,16]{1,2,0:T(8,128)(2,1)S(1)}, u32[]{:S(2)}, u32[]{:S(2)}) async-start(bf16[16,128,16]{1,2,0:T(8,128)(2,1)} %bitcast.27), calls=%async_computation.6 | async-start | bytes 131072 | tf_op jit(solution)/shard_map/all_to_all | solution.py:55
